TPU v7x, 32 devices: a whole 2x2x4 slice. The times are simulated.
32 devices in a mesh: st: 8 (over z, x), tp: 4 (over y, core).
Axes of the slice: x: 2, y: 2, z: 4, core: 2. Of those that a mesh axis runs over, the one named last changes fastest.
Arguments:
- tokens: bfloat16 [16384, 2048], P('st', 'tp'), may hold values from -48 to 48
- store: bfloat16 [256, 64, 2048], P('st'), may hold values from -48 to 48
- passage_holder_index: int32 [128, 2], P('st'), may hold values from 0 to 7, all different within a row; in each aligned block of 16 rows (0 to 15, 16 to 31, ...) at most 8 rows name the same one
- passage_slot: int32 [128, 2], P('st'), may hold values from 0 to 31
- query_weight: bfloat16 [2048, 1024], P(None, 'tp'), may hold values from -0.125 to 0.125
- key_matrix: bfloat16 [2048, 1024], P(None, 'tp'), may hold values from -0.125 to 0.125
- value_weight: bfloat16 [2048, 1024], P(None, 'tp'), may hold values from -0.125 to 0.125
- outer_gate: bfloat16 [2048, 1024], P(None, 'tp'), may hold values from -0.125 to 0.125
- inner_gate: bfloat16 [2048, 1024], P(None, 'tp'), may hold values from -0.125 to 0.125
- conv_input: bfloat16 [2048, 1024], P(None, 'tp'), may hold values from -0.125 to 0.125
- conv_taps: bfloat16 [3, 1024], P(None, 'tp'), may hold values from -3.5 to 3.5
- route_gate_projection: bfloat16 [2048, 2], replicated, may hold values from -0.125 to 0.125
- conv_out: bfloat16 [1024, 2048], P('tp'), may hold values from -0.1875 to 0.1875
- memory_out: bfloat16 [1024, 2048], P('tp'), may hold values from -0.1875 to 0.1875
Outputs:
- mixed: bfloat16 [16384, 2048], P(('st', 'tp'))
Inputs may be any that keep to these rules, and one draw needn't show every extreme that they name: `passage_holder_index`: each row names 2 different owners; among the rows of one index of st (16 aligned rows) no owner is named more than 8 times, a bound that some index of st reaches.
All inputs are finite; a program needn't handle non-finite values.
Results may differ from a plain program's by a relative error of at most 0.014.
Values may be sent and summed in bfloat16 or wider, within the bound.
A program may use at most 128 MiB of HBM per device.

v0:
```python
import functools

import jax
import jax.numpy as jnp
from jax import lax
from jax.experimental import pallas as pl
from jax.experimental.pallas import tpu as pltpu
from jax.sharding import PartitionSpec as P

HEAD_SIZE = 128
CONV_K = 3
SEQ_LEN = 256
BLOCK = 128
NPB = 2
PLEN = 64
CORES = 2
LANES = 128
MESH = pl.DeviceIdType.MESH


def flip(index, mask):
    result, bit = index, 1
    while bit <= mask:
        if mask & bit:
            result = result + bit * (1 - 2 * ((index // bit) % 2))
        bit *= 2
    return result


def aligned(start, size):
    return pl.ds(pl.multiple_of(start * size, size), size)


def fused_kernel(
    sizes,
    target_ref,
    mine_ref,
    ask_ref,
    tokens_ref,
    store_ref,
    key_ref,
    value_ref,
    query_ref,
    outer_ref,
    inner_ref,
    conv_ref,
    taps_ref,
    gate_ref,
    conv_out_ref,
    memory_out_ref,
    out_ref,
    tok,
    passages,
    in_weight,
    kv_weight,
    out_weight,
    total,
    queries,
    gates,
    result,
    wanted,
    wanted_smem,
    *rest,
):
    owners, team, heads, capacity, rows, feat = sizes
    chips = team // CORES
    own_rows = rows // team
    chunks = rows // SEQ_LEN
    refs = iter(rest)
    table = [next(refs) for _ in range(heads)]
    staged = [next(refs) for _ in range(heads)]
    served = [next(refs) for _ in range(heads)]
    branch = [next(refs) for _ in range(2 * heads)]
    moved = [next(refs) for _ in range(2 * heads)]
    (
        load_sem,
        store_sem,
        smem_sem,
        ask_send,
        ask_recv,
        near_send,
        near_recv,
        far_send,
        far_recv,
        pass_send,
        pass_recv,
        serve_send,
        serve_recv,
        row_send,
        row_recv,
        w_near_send,
        w_near_recv,
        w_far_send,
        w_far_recv,
        w_side_send,
        w_side_recv,
        w_pass_send,
        w_pass_recv,
        out_sem,
    ) = refs

    st = lax.axis_index("st")
    me = lax.axis_index("tp")
    chip, core = me // CORES, me % CORES
    partner = chip * CORES + 1 - core
    side = flip(st, 1)
    half = st % 2

    def up(k):
        return lax.rem(chip + k, chips) * CORES + core

    def down(k):
        return lax.rem(chip + chips - k, chips) * CORES + core

    def down_other(k):
        return lax.rem(chip + chips - k, chips) * CORES + 1 - core

    passage_rows = passages.shape[0]
    pieces = 4
    piece = passage_rows // pieces
    loads = []
    for h in range(heads):
        lanes = slice(h * HEAD_SIZE, (h + 1) * HEAD_SIZE)
        loads.append((key_ref.at[:, lanes], kv_weight.at[h, :, 0:HEAD_SIZE]))
        loads.append((value_ref.at[:, lanes], kv_weight.at[h, :, HEAD_SIZE : 2 * HEAD_SIZE]))
    kv_loads = len(loads)
    for i, ref in enumerate((query_ref, outer_ref, inner_ref, conv_ref)):
        loads.append((ref, in_weight.at[i]))
    loads.append((tokens_ref, tok.at[:, aligned(me, feat)]))
    token_loads = len(loads)
    for b, ref in enumerate((conv_out_ref, memory_out_ref)):
        for h in range(heads):
            loads.append(
                (
                    ref.at[h * HEAD_SIZE : (h + 1) * HEAD_SIZE, :],
                    out_weight.at[b, h, aligned(me, HEAD_SIZE), :],
                )
            )
    loads = [pltpu.make_async_copy(s, d, load_sem.at[i]) for i, (s, d) in enumerate(loads)]
    store_loads = [
        pltpu.make_async_copy(
            store_ref.at[i * piece : (i + 1) * piece, :],
            passages.at[i * piece : (i + 1) * piece, :],
            store_sem.at[i],
        )
        for i in range(pieces)
    ]
    for copy in loads[:kv_loads] + store_loads + loads[kv_loads:]:
        copy.start()

    barrier = pltpu.get_barrier_semaphore()
    for m in range(1, owners):
        pl.semaphore_signal(barrier, inc=1, device_id=(flip(st, m), me), device_id_type=MESH)
    for d in range(1, team):
        pl.semaphore_signal(
            barrier, inc=1, device_id=(st, lax.rem(me + d, team)), device_id_type=MESH
        )
    pl.semaphore_wait(barrier, owners - 1 + team - 1)

    def remote(src, dst, send, recv, device):
        return pltpu.make_async_remote_copy(
            src_ref=src,
            dst_ref=dst,
            send_sem=send,
            recv_sem=recv,
            device_id=device,
            device_id_type=MESH,
        )

    def ask(m, slot):
        return remote(
            ask_ref.at[flip(st, m)],
            wanted.at[slot],
            ask_send.at[m],
            ask_recv.at[m],
            (flip(st, m), me),
        )

    for m in range(owners - 1, 0, -1):
        ask(m, st).start()

    def far_copy(k, c, owner):
        return remote(
            tokens_ref.at[aligned(c, SEQ_LEN), :],
            tok.at[aligned(c, SEQ_LEN), aligned(owner, feat)],
            far_send.at[k - 1, c],
            far_recv.at[k - 1, c],
            (st, up(k)),
        )

    def near_copy(c, owner):
        return remote(
            tokens_ref.at[aligned(c, SEQ_LEN), :],
            tok.at[aligned(c, SEQ_LEN), aligned(owner, feat)],
            near_send.at[c],
            near_recv.at[c],
            (st, partner),
        )

    def pass_copy(k, c, owner):
        place = tok.at[aligned(c, SEQ_LEN), aligned(owner, feat)]
        return remote(
            place, place, pass_send.at[k - 1, c], pass_recv.at[k - 1, c], (st, partner)
        )

    @pl.loop(0, chunks)
    def _(c):
        for k in range(1, chips):
            far_copy(k, c, me).start()
        near_copy(c, me).start()

    def serve(h, m, slot):
        return remote(
            staged[h].at[flip(st, m)],
            served[h].at[aligned(slot, capacity)],
            serve_send.at[h, m],
            serve_recv.at[h, m],
            (flip(st, m), me),
        )

    for h in range(heads):
        loads[2 * h].wait()
        loads[2 * h + 1].wait()
        for i in range(pieces):
            if h == 0:
                store_loads[i].wait()
            found = jnp.dot(
                passages[i * piece : (i + 1) * piece, :],
                kv_weight[h],
                preferred_element_type=jnp.float32,
            ).astype(jnp.bfloat16)
            count = piece // PLEN
            table[h][i * count : (i + 1) * count] = found.reshape(count, PLEN, 2 * HEAD_SIZE)
        if h == 0:
            for m in range(1, owners):
                ask(m, flip(st, m)).wait_recv()
            numbers = pltpu.make_async_copy(wanted, wanted_smem, smem_sem)
            numbers.start()
            numbers.wait()
        for m in range(owners - 1, 0, -1):
            reader = flip(st, m)
            for c in range(capacity):
                staged[h][reader, c] = table[h][wanted_smem[reader, 0, c]]
            if m < owners - 1:
                serve(h, m + 1, st).start()
        for c in range(capacity):
            served[h][st * capacity + c] = table[h][mine_ref[st * capacity + c]]
        serve(h, 1, st).start()

    def w_near(owner):
        place = out_weight.at[:, :, aligned(owner, HEAD_SIZE), :]
        return remote(place, place, w_near_send, w_near_recv, (st, partner))

    def w_far(k, owner):
        place = out_weight.at[half, :, aligned(owner, HEAD_SIZE), :]
        return remote(place, place, w_far_send.at[k - 1], w_far_recv.at[k - 1], (st, up(k)))

    def w_side(k, owner, which):
        place = out_weight.at[which, :, aligned(owner, HEAD_SIZE), :]
        return remote(place, place, w_side_send.at[k - 1], w_side_recv.at[k - 1], (side, me))

    def w_pass(j, k, owner, which):
        place = out_weight.at[which, :, aligned(owner, HEAD_SIZE), :]
        return remote(
            place, place, w_pass_send.at[j, k - 1], w_pass_recv.at[j, k - 1], (st, partner)
        )

    for copy in loads[kv_loads:]:
        copy.wait()
    for k in range(1, chips):
        w_far(k, me).start()
    w_near(me).start()

    row_number = lax.broadcasted_iota(jnp.int32, (SEQ_LEN, 1), 0)
    taps = taps_ref[...].astype(jnp.float32)

    @pl.loop(0, chunks)
    def _(c):
        for k in range(1, chips):
            far_copy(k, c, down(k)).wait_recv()
            pass_copy(k, c, down(k)).start()
        near_copy(c, partner).wait_recv()
        for k in range(1, chips):
            pass_copy(k, c, down_other(k)).wait_recv()
        here = aligned(c, SEQ_LEN)
        x = tok[here, :]
        dot = functools.partial(jnp.dot, preferred_element_type=jnp.float32)
        queries[here, :] = dot(x, in_weight[0]).astype(jnp.bfloat16)
        mixed = dot(x, in_weight[2]) * dot(x, in_weight[3])
        filtered = jnp.zeros_like(mixed)
        for offset in range(CONV_K):
            back = CONV_K - 1 - offset
            shifted = mixed
            if back:
                shifted = jnp.where(row_number >= back, pltpu.roll(mixed, back, 0), 0.0)
            filtered = filtered + taps[offset : offset + 1, :] * shifted
        conv = (dot(x, in_weight[1]) * filtered).astype(jnp.bfloat16)
        for h in range(heads):
            branch[h][here, :] = conv[:, h * HEAD_SIZE : (h + 1) * HEAD_SIZE]

    def row_copy(i, d, source):
        owner = lax.rem(me + d, team)
        return remote(
            branch[i].at[aligned(owner, own_rows), :],
            moved[i].at[:, aligned(source, HEAD_SIZE)],
            row_send.at[i, d],
            row_recv.at[i, d],
            (st, owner),
        )

    def keep_rows(i):
        moved[i][:, aligned(me, HEAD_SIZE)] = branch[i][aligned(me, own_rows), :]

    def wait_rows(i):
        for d in range(1, team):
            row_copy(i, d, lax.rem(me + team - d, team)).wait_recv()

    for i in range(heads):
        for d in range(1, team):
            row_copy(i, d, me).start()
        keep_rows(i)

    gates[...] = jax.nn.sigmoid(
        jnp.dot(tok[aligned(me, own_rows), :], gate_ref[...], preferred_element_type=jnp.float32)
    )

    order = [d for d in range(1, team) if d % CORES == 0]
    order += [d for d in range(1, team) if d % CORES]
    blocks = own_rows // BLOCK
    tile = 512
    tiles = out_weight.shape[3] // tile

    def attention(h):
        for m in range(1, owners):
            serve(h, m, flip(st, m)).wait_recv()

        def owner_rows(d):
            owner = lax.rem(me + d, team)
            for b in range(blocks):
                number = owner * blocks + b
                here = aligned(number, BLOCK)
                joined = jnp.concatenate(
                    [served[h][target_ref[number * NPB + j]] for j in range(NPB)], axis=0
                )
                scores = lax.dot_general(
                    queries[here, h * HEAD_SIZE : (h + 1) * HEAD_SIZE],
                    joined[:, :HEAD_SIZE],
                    (((1,), (1,)), ((), ())),
                    preferred_element_type=jnp.float32,
                ) * HEAD_SIZE ** (-0.5)
                scores = jnp.exp(scores - jnp.max(scores, axis=1, keepdims=True))
                weights = (scores / jnp.sum(scores, axis=1, keepdims=True)).astype(jnp.bfloat16)
                branch[heads + h][here, :] = jnp.dot(
                    weights, joined[:, HEAD_SIZE:], preferred_element_type=jnp.float32
                ).astype(jnp.bfloat16)

        for d in order:
            owner_rows(d)
            row_copy(heads + h, d, me).start()
        owner_rows(0)
        keep_rows(heads + h)

    for h in range(heads):
        attention(h)
        if h == 0:
            for k in range(1, chips):
                w_far(k, down(k)).wait_recv()
                w_side(k, down(k), half).start()
                w_pass(0, k, down(k), half).start()
            for k in range(1, chips):
                w_side(k, down(k), 1 - half).wait_recv()
                w_pass(1, k, down(k), 1 - half).start()
            w_near(partner).wait_recv()
            for k in range(1, chips):
                w_pass(0, k, down_other(k), half).wait_recv()
                w_pass(1, k, down_other(k), 1 - half).wait_recv()
            for i in range(heads):
                wait_rows(i)

            @pl.loop(0, tiles)
            def _(n):
                lanes = aligned(n, tile)
                value = 0.0
                for i in range(heads):
                    value = value + jnp.dot(
                        moved[i][...],
                        out_weight[0, i, :, lanes],
                        preferred_element_type=jnp.float32,
                    )
                total[:, lanes] = gates[:, 0:1] * value

        wait_rows(heads + h)

        @pl.loop(0, tiles)
        def _(n):
            lanes = aligned(n, tile)
            value = total[:, lanes] + gates[:, 1:2] * jnp.dot(
                moved[heads + h][...],
                out_weight[1, h, :, lanes],
                preferred_element_type=jnp.float32,
            )
            if h < heads - 1:
                total[:, lanes] = value
            else:
                result[:, lanes] = value.astype(jnp.bfloat16)

    written = pltpu.make_async_copy(result, out_ref, out_sem)
    written.start()

    for m in range(1, owners):
        ask(m, st).wait_send()
        for h in range(heads):
            serve(h, m, st).wait_send()

    @pl.loop(0, chunks)
    def _(c):
        for k in range(1, chips):
            far_copy(k, c, me).wait_send()
            pass_copy(k, c, down(k)).wait_send()
        near_copy(c, me).wait_send()

    for k in range(1, chips):
        w_far(k, me).wait_send()
        w_side(k, down(k), half).wait_send()
        w_pass(0, k, down(k), half).wait_send()
        w_pass(1, k, down(k), 1 - half).wait_send()
    w_near(me).wait_send()
    for i in range(2 * heads):
        for d in range(1, team):
            row_copy(i, d, me).wait_send()
    written.wait()


def local(
    tokens,
    store,
    passage_holder_index,
    passage_slot,
    query_weight,
    key_matrix,
    value_weight,
    outer_gate,
    inner_gate,
    conv_input,
    conv_taps,
    route_gate_projection,
    conv_out,
    memory_out,
):
    rows, feat = tokens.shape
    head_width = query_weight.shape[1]
    heads = head_width // HEAD_SIZE
    width = conv_out.shape[1]
    team = lax.axis_size("tp")
    owners = lax.axis_size("st")
    own_rows = rows // team
    depth = team * HEAD_SIZE
    chips = team // CORES
    chunks = rows // SEQ_LEN

    names = passage_holder_index.reshape(-1)
    slots = passage_slot.reshape(-1)
    count = names.shape[0]
    capacity = max(2, 2 * count // owners)
    earlier = jnp.arange(count)[None, :] < jnp.arange(count)[:, None]
    position = jnp.sum(
        jnp.where(earlier & (names[:, None] == names[None, :]), 1, 0), axis=1, dtype=jnp.int32
    )
    target = names * capacity + position
    places = jnp.arange(owners * capacity, dtype=jnp.int32)
    mine = jnp.sum(
        jnp.where(target[None, :] == places[:, None], slots[None, :], 0), axis=1, dtype=jnp.int32
    )
    ask = jnp.pad(mine.reshape(owners, 1, capacity), ((0, 0), (0, 7), (0, LANES - capacity)))
    gate_weight = jnp.pad(route_gate_projection, ((0, 0), (0, LANES - 2)))

    flat_rows = store.reshape(-1, store.shape[-1])
    held = store.shape[0]
    bf16, f32 = jnp.bfloat16, jnp.float32
    dma = pltpu.SemaphoreType.DMA
    scratch = [
        pltpu.VMEM((rows, team * feat), bf16),
        pltpu.VMEM(flat_rows.shape, bf16),
        pltpu.VMEM((4, team * feat, head_width), bf16),
        pltpu.VMEM((heads, team * feat, 2 * HEAD_SIZE), bf16),
        pltpu.VMEM((2, heads, depth, width), bf16),
        pltpu.VMEM((own_rows, width), f32),
        pltpu.VMEM((rows, head_width), bf16),
        pltpu.VMEM((own_rows, LANES), f32),
        pltpu.VMEM((own_rows, width), bf16),
        pltpu.VMEM((owners, 8, LANES), jnp.int32),
        pltpu.SMEM((owners, 8, LANES), jnp.int32),
    ]
    scratch += [pltpu.VMEM((held, PLEN, 2 * HEAD_SIZE), bf16)] * heads
    scratch += [pltpu.VMEM((owners, capacity, PLEN, 2 * HEAD_SIZE), bf16)] * heads
    scratch += [pltpu.VMEM((owners * capacity, PLEN, 2 * HEAD_SIZE), bf16)] * heads
    scratch += [pltpu.VMEM((rows, HEAD_SIZE), bf16)] * (2 * heads)
    scratch += [pltpu.VMEM((own_rows, depth), bf16)] * (2 * heads)
    scratch += [
        dma((4 * heads + 5,)),
        dma((4,)),
        dma,
        dma((owners,)),
        dma((owners,)),
        dma((chunks,)),
        dma((chunks,)),
        dma((chips - 1, chunks)),
        dma((chips - 1, chunks)),
        dma((chips - 1, chunks)),
        dma((chips - 1, chunks)),
        dma((heads, owners)),
        dma((heads, owners)),
        dma((2 * heads, team)),
        dma((2 * heads, team)),
        dma,
        dma,
        dma((chips - 1,)),
        dma((chips - 1,)),
        dma((chips - 1,)),
        dma((chips - 1,)),
        dma((2, chips - 1)),
        dma((2, chips - 1)),
        dma,
    ]
    smem = pl.BlockSpec(memory_space=pltpu.SMEM)
    vmem = pl.BlockSpec(memory_space=pltpu.VMEM)
    hbm = pl.BlockSpec(memory_space=pl.ANY)
    return pl.pallas_call(
        functools.partial(fused_kernel, (owners, team, heads, capacity, rows, feat)),
        out_shape=jax.ShapeDtypeStruct((own_rows, width), bf16),
        in_specs=[smem, smem, vmem] + [hbm] * 8 + [vmem, vmem] + [hbm] * 2,
        out_specs=hbm,
        scratch_shapes=scratch,
        compiler_params=pltpu.CompilerParams(
            collective_id=0, has_side_effects=True, vmem_limit_bytes=66_000_000
        ),
    )(
        target,
        mine,
        ask,
        tokens,
        flat_rows,
        key_matrix,
        value_weight,
        query_weight,
        outer_gate,
        inner_gate,
        conv_input,
        conv_taps,
        gate_weight,
        conv_out,
        memory_out,
    )


def solution(mesh):
    return jax.shard_map(
        local,
        mesh=mesh,
        in_specs=(
            P("st", "tp"),
            P("st", None, None),
            P("st", None),
            P("st", None),
            P(None, "tp"),
            P(None, "tp"),
            P(None, "tp"),
            P(None, "tp"),
            P(None, "tp"),
            P(None, "tp"),
            P(None, "tp"),
            P(),
            P("tp", None),
            P("tp", None),
        ),
        out_specs=P(("st", "tp"), None),
        check_vma=False,
    )
```

profile of v0, /device:TPU:0, one launch (start us, length us, event | category | flops | bytes accessed | tf_op | source)
XLA Modules:
  0.0 148.4 jit_solution(17609158795527823753)
XLA Ops:
  0.0 0.8 copy.23
  0.8 0.1 reshape.20
  0.8 0.2 select_reduce_fusion.1
  1.0 0.0 copy-start.1
  1.0 0.8 copy.24
  1.8 0.1 broadcast_in_dim.28
  1.9 0.1 select_reduce_fusion.mine_ref
  2.0 0.0 copy-start
  2.0 0.1 reshape.21
  2.1 0.6 pad.8.ask_ref
  2.7 1.0 copy.26
  3.7 0.9 pad.9.gate_ref
  4.6 0.0 copy-done.1
  4.6 0.0 copy-done
  4.6 140.6 %shard_map.136 = bf16[512,2048]{1,0:T(8,128)(2,1)} custom-call(s32[32]{0:T(128)} %copy-done.1, s32[64]{0:T(128)} %copy-done, s32[8,8,128]{2,1,0:T(8,128)} %pad.8.ask_ref, bf16[2048,512]{1,0:T(8,128)(2,1)} %tokens_ref.1, bf16[2048,2048]{1,0:T(8,128)(2,1)} %bitcast.2, bf16[2048,256]{1,0:T(8,128)(2,1)} %key_ref.1, bf16[2048,256]{1,0:T(8,128)(2,1)} %value_ref.1, ...), custom_call_target="tpu_custom_call" | custom-call | tf_op jit(solution)/shard_map/pallas_call | solution.py:528
  145.2 3.2 %copy.28 = bf16[512,2048]{1,0:T(8,128)(2,1)} copy(bf16[512,2048]{1,0:T(8,128)(2,1)} %shard_map.136) | data formatting | bytes 4194304
  (1 shorter events, 0.0 us)
Async XLA Ops:
  1.0 3.6 %copy-start.1 = (s32[32]{0:T(128)}, s32[32]{0:T(128)S(1)}, u32[]{:S(2)}) copy-start(s32[32]{0:T(128)S(1)} %multiply_add_fusion.target_ref) | copy-start | bytes 388
  2.0 2.6 %copy-start = (s32[64]{0:T(128)}, s32[64]{0:T(128)S(1)}, u32[]{:S(2)}) copy-start(s32[64]{0:T(128)S(1)} %select_reduce_fusion.mine_ref) | copy-start | bytes 772
where the time goes:
time: 149 us; the launch traced here: 148 us
  Pallas kernels  141 us (95%)
  local copies, waits for them, and re-layouts  7.45 us (5%)
    pallas_call x1, Pallas kernels, local(): pl.pallas_call(functools.partial(fused_kernel, (owners, team, heads, capa...  141 us
    unnamed x8, local copies, waits for them, and re-layouts  5.69 us

commit v1 on v0

v1 whole, which is shorter than its diff:
```python
import functools

import jax
import jax.numpy as jnp
from jax import lax
from jax.experimental import pallas as pl
from jax.experimental.pallas import tpu as pltpu
from jax.sharding import PartitionSpec as P

HEAD_SIZE = 128
CONV_K = 3
SEQ_LEN = 256
BLOCK = 128
NPB = 2
PLEN = 64
CORES = 2
LANES = 128
LOG2_E = 1.4426950408889634
MESH = pl.DeviceIdType.MESH


def flip(index, mask):
    result, bit = index, 1
    while bit <= mask:
        if mask & bit:
            result = result + bit * (1 - 2 * ((index // bit) % 2))
        bit *= 2
    return result


def aligned(start, size):
    return pl.ds(pl.multiple_of(start * size, size), size)


def fused_kernel(
    sizes,
    names_ref,
    slots_ref,
    tokens_ref,
    store_ref,
    key_ref,
    value_ref,
    query_ref,
    outer_ref,
    inner_ref,
    conv_ref,
    taps_ref,
    gate_ref,
    conv_out_ref,
    memory_out_ref,
    out_ref,
    tok,
    passages,
    in_weight,
    kv_weight,
    out_weight,
    total,
    queries,
    gates,
    powers,
    asked,
    wanted,
    target,
    *rest,
):
    owners, team, heads, capacity, rows, feat = sizes
    chips = team // CORES
    own_rows = rows // team
    chunks = rows // SEQ_LEN
    refs = iter(rest)
    table = [next(refs) for _ in range(2 * heads)]
    staged = [next(refs) for _ in range(2 * heads)]
    served = [next(refs) for _ in range(2 * heads)]
    branch = [next(refs) for _ in range(2 * heads)]
    moved = [next(refs) for _ in range(2 * heads)]
    (
        load_sem,
        store_sem,
        smem_sem,
        ask_send,
        ask_recv,
        near_send,
        near_recv,
        far_send,
        far_recv,
        pass_send,
        pass_recv,
        serve_send,
        serve_recv,
        row_send,
        row_recv,
        w_near_send,
        w_near_recv,
        w_far_send,
        w_far_recv,
        w_side_send,
        w_side_recv,
        w_pass_send,
        w_pass_recv,
    ) = refs

    st = lax.axis_index("st")
    me = lax.axis_index("tp")
    chip, core = me // CORES, me % CORES
    partner = chip * CORES + 1 - core
    side = flip(st, 1)
    half = st % 2

    def up(k):
        return lax.rem(chip + k, chips) * CORES + core

    def down(k):
        return lax.rem(chip + chips - k, chips) * CORES + core

    def down_other(k):
        return lax.rem(chip + chips - k, chips) * CORES + 1 - core

    passage_rows = passages.shape[0]
    pieces = 4
    piece = passage_rows // pieces
    loads = []
    for h in range(heads):
        lanes = slice(h * HEAD_SIZE, (h + 1) * HEAD_SIZE)
        loads.append((key_ref.at[:, lanes], kv_weight.at[h, :, 0:HEAD_SIZE]))
        loads.append((value_ref.at[:, lanes], kv_weight.at[h, :, HEAD_SIZE : 2 * HEAD_SIZE]))
    kv_loads = len(loads)
    for i, ref in enumerate((query_ref, outer_ref, inner_ref, conv_ref)):
        loads.append((ref, in_weight.at[i]))
    loads.append((tokens_ref, tok.at[:, aligned(me, feat)]))
    token_loads = len(loads)
    for b, ref in enumerate((conv_out_ref, memory_out_ref)):
        for h in range(heads):
            loads.append(
                (
                    ref.at[h * HEAD_SIZE : (h + 1) * HEAD_SIZE, :],
                    out_weight.at[b, h, aligned(me, HEAD_SIZE), :],
                )
            )
    loads = [pltpu.make_async_copy(s, d, load_sem.at[i]) for i, (s, d) in enumerate(loads)]
    store_loads = [
        pltpu.make_async_copy(
            store_ref.at[i * piece : (i + 1) * piece, :],
            passages.at[i * piece : (i + 1) * piece, :],
            store_sem.at[i],
        )
        for i in range(pieces)
    ]
    for copy in loads[:2] + store_loads + loads[token_loads:]:
        copy.start()

    barrier = pltpu.get_barrier_semaphore()
    for m in range(1, owners):
        pl.semaphore_signal(barrier, inc=1, device_id=(flip(st, m), me), device_id_type=MESH)
    for d in range(1, team):
        pl.semaphore_signal(
            barrier, inc=1, device_id=(st, lax.rem(me + d, team)), device_id_type=MESH
        )

    lane = lax.broadcasted_iota(jnp.int32, (owners, LANES), 1)
    row = lax.broadcasted_iota(jnp.int32, (owners, LANES), 0)
    requests = [(j, b) for j in range(NPB) for b in range(names_ref.shape[1])]
    filled = jnp.zeros((owners, LANES), jnp.int32)
    asks = jnp.zeros((owners, LANES), jnp.int32)
    for j, b in requests:
        hit = row == names_ref[j, b]
        asks = jnp.where(hit & (lane == filled), slots_ref[j, b], asks)
        filled = jnp.where(hit, filled + 1, filled)
    for o in range(owners):
        asked[o, 0:1, :] = asks[o : o + 1, :]

    def project(h, i):
        found = jnp.dot(
            passages[i * piece : (i + 1) * piece, :],
            kv_weight[h],
            preferred_element_type=jnp.float32,
        ).astype(jnp.bfloat16)
        count = piece // PLEN
        for j in range(2):
            part = found[:, j * HEAD_SIZE : (j + 1) * HEAD_SIZE]
            table[2 * h + j][i * count : (i + 1) * count] = part.reshape(count, PLEN, HEAD_SIZE)

    def project_half(part):
        mine = range(part * pieces // 2, (part + 1) * pieces // 2)
        for i in mine:
            store_loads[i].wait()
        for i in mine:
            project(0, i)

    pl.semaphore_wait(barrier, owners - 1 + team - 1)

    def remote(src, dst, send, recv, device):
        return pltpu.make_async_remote_copy(
            src_ref=src,
            dst_ref=dst,
            send_sem=send,
            recv_sem=recv,
            device_id=device,
            device_id_type=MESH,
        )

    def ask(m, slot):
        return remote(
            asked.at[flip(st, m)],
            wanted.at[slot],
            ask_send.at[m],
            ask_recv.at[m],
            (flip(st, m), me),
        )

    for m in range(owners - 1, 0, -1):
        ask(m, st).start()
    loads[0].wait()
    loads[1].wait()
    project_half(0)

    def far_copy(k, c, owner):
        return remote(
            tokens_ref.at[aligned(c, SEQ_LEN), :],
            tok.at[aligned(c, SEQ_LEN), aligned(owner, feat)],
            far_send.at[k - 1, c],
            far_recv.at[k - 1, c],
            (st, up(k)),
        )

    def near_copy(c, owner):
        return remote(
            tokens_ref.at[aligned(c, SEQ_LEN), :],
            tok.at[aligned(c, SEQ_LEN), aligned(owner, feat)],
            near_send.at[c],
            near_recv.at[c],
            (st, partner),
        )

    def pass_copy(k, c, owner):
        place = tok.at[aligned(c, SEQ_LEN), aligned(owner, feat)]
        return remote(
            place, place, pass_send.at[k - 1, c], pass_recv.at[k - 1, c], (st, partner)
        )

    def w_near(owner):
        place = out_weight.at[:, :, aligned(owner, HEAD_SIZE), :]
        return remote(place, place, w_near_send, w_near_recv, (st, partner))

    def w_far(k, owner):
        place = out_weight.at[half, :, aligned(owner, HEAD_SIZE), :]
        return remote(place, place, w_far_send.at[k - 1], w_far_recv.at[k - 1], (st, up(k)))

    def w_side(k, owner, which):
        place = out_weight.at[which, :, aligned(owner, HEAD_SIZE), :]
        return remote(place, place, w_side_send.at[k - 1], w_side_recv.at[k - 1], (side, me))

    def w_pass(j, k, owner, which):
        place = out_weight.at[which, :, aligned(owner, HEAD_SIZE), :]
        return remote(
            place, place, w_pass_send.at[j, k - 1], w_pass_recv.at[j, k - 1], (st, partner)
        )

    for copy in loads[token_loads:]:
        copy.wait()
    for k in range(1, chips):
        w_far(k, me).start()
    w_near(me).start()

    @pl.loop(0, chunks)
    def _(c):
        for k in range(1, chips):
            far_copy(k, c, me).start()
        near_copy(c, me).start()

    def serve(i, m, slot):
        return remote(
            staged[i].at[flip(st, m)],
            served[i].at[aligned(slot, capacity)],
            serve_send.at[i, m],
            serve_recv.at[i, m],
            (flip(st, m), me),
        )

    def pass_weights():
        for k in range(1, chips):
            w_far(k, down(k)).wait_recv()
            w_side(k, down(k), half).start()
            w_pass(0, k, down(k), half).start()

    project_half(1)
    for copy in loads[2:token_loads]:
        copy.start()
    own_asks = pltpu.make_async_copy(asked.at[st], wanted.at[st], smem_sem)
    own_asks.start()
    for m in range(1, owners):
        ask(m, flip(st, m)).wait_recv()
    own_asks.wait()
    for h in range(heads):
        if h:
            loads[2 * h].wait()
            loads[2 * h + 1].wait()
            for i in range(pieces):
                project(h, i)
        if h == 1:
            pass_weights()
        for i in (2 * h, 2 * h + 1):
            for m in range(owners - 1, 0, -1):
                reader = flip(st, m)
                for c in range(capacity):
                    staged[i][reader, c] = table[i][wanted[reader, 0, c]]
                if m < owners - 1:
                    serve(i, m + 1, st).start()
            for c in range(capacity):
                served[i][st * capacity + c] = table[i][wanted[st, 0, c]]
            serve(i, 1, st).start()
    if heads == 1:
        pass_weights()

    for f, (j, b) in enumerate(requests):
        name = names_ref[j, b]
        place = name * capacity
        for i, a in requests[:f]:
            place = place + jnp.where(names_ref[i, a] == name, 1, 0)
        target[b * NPB + j] = place

    for copy in loads[kv_loads:token_loads]:
        copy.wait()

    row_number = lax.broadcasted_iota(jnp.int32, (SEQ_LEN, 1), 0)
    taps = taps_ref[...].astype(jnp.float32)

    @pl.loop(0, chunks)
    def _(c):
        for k in range(1, chips):
            far_copy(k, c, down(k)).wait_recv()
            pass_copy(k, c, down(k)).start()
        near_copy(c, partner).wait_recv()
        for k in range(1, chips):
            pass_copy(k, c, down_other(k)).wait_recv()
        here = aligned(c, SEQ_LEN)
        x = tok[here, :]
        dot = functools.partial(jnp.dot, preferred_element_type=jnp.float32)
        queries[here, :] = dot(x, in_weight[0]).astype(jnp.bfloat16)
        mixed = dot(x, in_weight[2]) * dot(x, in_weight[3])
        filtered = jnp.zeros_like(mixed)
        for offset in range(CONV_K):
            back = CONV_K - 1 - offset
            shifted = mixed
            if back:
                shifted = jnp.where(row_number >= back, pltpu.roll(mixed, back, 0), 0.0)
            filtered = filtered + taps[offset : offset + 1, :] * shifted
        conv = (dot(x, in_weight[1]) * filtered).astype(jnp.bfloat16)
        for h in range(heads):
            branch[h][here, :] = conv[:, h * HEAD_SIZE : (h + 1) * HEAD_SIZE]

    others = [place(k) for k in range(1, chips) for place in (down, down_other)] + [partner]

    def row_send_copy(i, owner):
        d = lax.rem(owner - me + team, team)
        return remote(
            branch[i].at[aligned(owner, own_rows), :],
            moved[i].at[:, aligned(me, HEAD_SIZE)],
            row_send.at[i, d],
            row_recv.at[i, d],
            (st, owner),
        )

    def row_recv_copy(i, source):
        d = lax.rem(me - source + team, team)
        return remote(
            branch[i].at[aligned(source, own_rows), :],
            moved[i].at[:, aligned(source, HEAD_SIZE)],
            row_send.at[i, d],
            row_recv.at[i, d],
            (st, source),
        )

    def keep_rows(i):
        moved[i][:, aligned(me, HEAD_SIZE)] = branch[i][aligned(me, own_rows), :]

    def wait_rows(i):
        for source in others:
            row_recv_copy(i, source).wait_recv()

    for i in range(heads):
        for owner in others:
            row_send_copy(i, owner).start()
        keep_rows(i)

    gates[...] = jax.nn.sigmoid(
        lax.dot_general(
            tok[aligned(me, own_rows), :],
            gate_ref[...],
            (((1,), (1,)), ((), ())),
            preferred_element_type=jnp.float32,
        )
    )

    blocks = own_rows // BLOCK
    tile = 512
    tiles = out_weight.shape[3] // tile

    ones = jnp.ones((NPB * PLEN, HEAD_SIZE), jnp.bfloat16)

    def attention(h):
        def owner_powers(owner):
            for b in range(blocks):
                n = owner * blocks + b
                keys = jnp.concatenate(
                    [served[2 * h][target[n * NPB + j]] for j in range(NPB)], axis=0
                )
                scores = lax.dot_general(
                    queries[aligned(n, BLOCK), h * HEAD_SIZE : (h + 1) * HEAD_SIZE],
                    keys,
                    (((1,), (1,)), ((), ())),
                    preferred_element_type=jnp.float32,
                )
                scores = scores - jnp.max(scores, axis=1, keepdims=True)
                powers[aligned(n, BLOCK), :] = jnp.exp2(
                    scores * (HEAD_SIZE**-0.5 * LOG2_E)
                ).astype(jnp.bfloat16)

        def owner_rows(owner):
            numbers = [owner * blocks + b for b in range(blocks)]
            values = [
                jnp.concatenate(
                    [served[2 * h + 1][target[n * NPB + j]] for j in range(NPB)], axis=0
                )
                for n in numbers
            ]
            sums = [
                jnp.dot(
                    powers[aligned(n, BLOCK), :],
                    jnp.concatenate([value, ones], axis=1),
                    preferred_element_type=jnp.float32,
                )
                for n, value in zip(numbers, values)
            ]
            for n, both in zip(numbers, sums):
                branch[heads + h][aligned(n, BLOCK), :] = (
                    both[:, :HEAD_SIZE] / both[:, HEAD_SIZE:]
                ).astype(jnp.bfloat16)

        for m in range(1, owners):
            serve(2 * h, m, flip(st, m)).wait_recv()

        @pl.loop(0, team)
        def _(owner):
            owner_powers(owner)

        for m in range(1, owners):
            serve(2 * h + 1, m, flip(st, m)).wait_recv()
        for owner in others:
            owner_rows(owner)
            row_send_copy(heads + h, owner).start()
        owner_rows(me)
        keep_rows(heads + h)

    def add_memory(h, near, far, last):
        def add_tile(n):
            lanes = aligned(n, tile)
            value = total[:, lanes]
            for k in range(0 if near else 1, chips if far else 1):
                rows_of = aligned(lax.rem(chip + k, chips), CORES * HEAD_SIZE)
                value = value + gates[:, 1:2] * jnp.dot(
                    moved[heads + h][:, rows_of],
                    out_weight[1, h, rows_of, lanes],
                    preferred_element_type=jnp.float32,
                )
            if last:
                out_ref[:, lanes] = value.astype(jnp.bfloat16)
            else:
                total[:, lanes] = value

        if last:
            for n in range(tiles):
                add_tile(n)
        else:
            pl.loop(0, tiles)(add_tile)

    for k in range(1, chips):
        w_side(k, down(k), 1 - half).wait_recv()
        w_pass(1, k, down(k), 1 - half).start()

    def drain():
        for m in range(1, owners):
            ask(m, st).wait_send()
            for i in range(2 * heads):
                serve(i, m, st).wait_send()

        @pl.loop(0, chunks)
        def _(c):
            for k in range(1, chips):
                far_copy(k, c, me).wait_send()
                pass_copy(k, c, down(k)).wait_send()
            near_copy(c, me).wait_send()

        for k in range(1, chips):
            w_far(k, me).wait_send()
            w_side(k, down(k), half).wait_send()
            w_pass(0, k, down(k), half).wait_send()
            w_pass(1, k, down(k), 1 - half).wait_send()
        w_near(me).wait_send()

    for h in range(heads):
        attention(h)
        if h == 0:
            w_near(partner).wait_recv()
            for k in range(1, chips):
                w_pass(0, k, down_other(k), half).wait_recv()
                w_pass(1, k, down_other(k), 1 - half).wait_recv()
            for i in range(heads):
                wait_rows(i)

            @pl.loop(0, tiles)
            def _(n):
                lanes = aligned(n, tile)
                value = 0.0
                for i in range(heads):
                    value = value + jnp.dot(
                        moved[i][...],
                        out_weight[0, i, :, lanes],
                        preferred_element_type=jnp.float32,
                    )
                total[:, lanes] = gates[:, 0:1] * value

        if h < heads - 1:
            wait_rows(heads + h)
            add_memory(h, True, True, False)
        else:
            row_recv_copy(heads + h, partner).wait_recv()
            add_memory(h, True, False, False)
            drain()
            for source in others[:-1]:
                row_recv_copy(heads + h, source).wait_recv()
            add_memory(h, False, True, True)

    for i in range(2 * heads):
        for owner in others:
            row_send_copy(i, owner).wait_send()


def local(
    tokens,
    store,
    passage_holder_index,
    passage_slot,
    query_weight,
    key_matrix,
    value_weight,
    outer_gate,
    inner_gate,
    conv_input,
    conv_taps,
    route_gate_projection,
    conv_out,
    memory_out,
):
    rows, feat = tokens.shape
    head_width = query_weight.shape[1]
    heads = head_width // HEAD_SIZE
    width = conv_out.shape[1]
    team = lax.axis_size("tp")
    owners = lax.axis_size("st")
    own_rows = rows // team
    depth = team * HEAD_SIZE
    chips = team // CORES
    chunks = rows // SEQ_LEN

    count = passage_holder_index.size
    capacity = max(2, 2 * count // owners)
    flat_rows = store.reshape(-1, store.shape[-1])
    held = store.shape[0]
    bf16, f32 = jnp.bfloat16, jnp.float32
    dma = pltpu.SemaphoreType.DMA
    scratch = [
        pltpu.VMEM((rows, team * feat), bf16),
        pltpu.VMEM(flat_rows.shape, bf16),
        pltpu.VMEM((4, team * feat, head_width), bf16),
        pltpu.VMEM((heads, team * feat, 2 * HEAD_SIZE), bf16),
        pltpu.VMEM((2, heads, depth, width), bf16),
        pltpu.VMEM((own_rows, width), f32),
        pltpu.VMEM((rows, head_width), bf16),
        pltpu.VMEM((own_rows, 2), f32),
        pltpu.VMEM((rows, NPB * PLEN), bf16),
        pltpu.VMEM((owners, 8, LANES), jnp.int32),
        pltpu.SMEM((owners, 8, LANES), jnp.int32),
        pltpu.SMEM((count,), jnp.int32),
    ]
    scratch += [pltpu.VMEM((held, PLEN, HEAD_SIZE), bf16)] * (2 * heads)
    scratch += [pltpu.VMEM((owners, capacity, PLEN, HEAD_SIZE), bf16)] * (2 * heads)
    scratch += [pltpu.VMEM((owners * capacity, PLEN, HEAD_SIZE), bf16)] * (2 * heads)
    scratch += [pltpu.VMEM((rows, HEAD_SIZE), bf16)] * (2 * heads)
    scratch += [pltpu.VMEM((own_rows, depth), bf16)] * (2 * heads)
    scratch += [
        dma((4 * heads + 5,)),
        dma((4,)),
        dma,
        dma((owners,)),
        dma((owners,)),
        dma((chunks,)),
        dma((chunks,)),
        dma((chips - 1, chunks)),
        dma((chips - 1, chunks)),
        dma((chips - 1, chunks)),
        dma((chips - 1, chunks)),
        dma((2 * heads, owners)),
        dma((2 * heads, owners)),
        dma((2 * heads, team)),
        dma((2 * heads, team)),
        dma,
        dma,
        dma((chips - 1,)),
        dma((chips - 1,)),
        dma((chips - 1,)),
        dma((chips - 1,)),
        dma((2, chips - 1)),
        dma((2, chips - 1)),
    ]
    smem = pl.BlockSpec(memory_space=pltpu.SMEM)
    vmem = pl.BlockSpec(memory_space=pltpu.VMEM)
    hbm = pl.BlockSpec(memory_space=pltpu.HBM)
    return pl.pallas_call(
        functools.partial(fused_kernel, (owners, team, heads, capacity, rows, feat)),
        out_shape=pltpu.VMEM((own_rows, width), bf16),
        in_specs=[smem, smem] + [hbm] * 8 + [vmem, vmem] + [hbm] * 2,
        out_specs=vmem,
        scratch_shapes=scratch,
        compiler_params=pltpu.CompilerParams(
            collective_id=0, has_side_effects=True, vmem_limit_bytes=56 * 1024 * 1024
        ),
    )(
        passage_holder_index.T,
        passage_slot.T,
        tokens,
        flat_rows,
        key_matrix,
        value_weight,
        query_weight,
        outer_gate,
        inner_gate,
        conv_input,
        conv_taps,
        route_gate_projection.T,
        conv_out,
        memory_out,
    )


def solution(mesh):
    return jax.shard_map(
        local,
        mesh=mesh,
        in_specs=(
            P("st", "tp"),
            P("st", None, None),
            P("st", None),
            P("st", None),
            P(None, "tp"),
            P(None, "tp"),
            P(None, "tp"),
            P(None, "tp"),
            P(None, "tp"),
            P(None, "tp"),
            P(None, "tp"),
            P(),
            P("tp", None),
            P("tp", None),
        ),
        out_specs=P(("st", "tp"), None),
        check_vma=False,
    )
```

time: 149 us -> 112 us (0.75)
  Pallas kernels: 141 us -> 110 us
  local copies, waits for them, and re-layouts: 7.45 us -> 1.32 us
    pallas_call x1, Pallas kernels: 141 us -> 110 us  [local(): pl.pallas_call(functools.partial(fused_kernel, (owners, team, heads, capa...]
    unnamed x8 -> x1, local copies, waits for them, and re-layouts: 5.69 us -> 1.32 us
    pad x2 -> x0, local copies, waits for them, and re-layouts: 1.52 us -> none  [the longest x1 0.9 us: local(): gate_weight = jnp.pad(route_gate_projection, ((0, 0), (0, LANES - 2)))]
where the time goes in v1:
time: 112 us; the launch traced here: 111 us
  Pallas kernels  110 us (98%)
  local copies, waits for them, and re-layouts  1.32 us (1%)
    pallas_call x1, Pallas kernels, local(): pl.pallas_call(functools.partial(fused_kernel, (owners, team, heads, capa...  110 us

profile of v1, /device:TPU:0, one launch (start us, length us, event | category | flops | bytes accessed | tf_op | source)
XLA Modules:
  0.0 110.9 jit_solution(2436459663129640149)
XLA Ops:
  0.0 109.6 %shard_map.136 = bf16[512,2048]{1,0:T(8,128)(2,1)S(1)} custom-call(s32[2,16]{1,0:T(2,128)} %bitcast.6, s32[2,16]{1,0:T(2,128)} %bitcast.7, bf16[2048,512]{1,0:T(8,128)(2,1)} %tokens_ref.1, bf16[2048,2048]{1,0:T(8,128)(2,1)} %bitcast.4, bf16[2048,256]{1,0:T(8,128)(2,1)} %key_ref.1, bf16[2048,256]{1,0:T(8,128)(2,1)} %value_ref.1, bf16[2048,256]{1,0:T(8,128)(2,1)} %query_ref.1, ...), custom_call_target="tpu_custom_call" | custom-call | tf_op jit(solution)/shard_map/pallas_call | solution.py:618
  109.6 1.3 %copy.16 = bf16[512,2048]{1,0:T(8,128)(2,1)} copy(bf16[512,2048]{1,0:T(8,128)(2,1)S(1)} %shard_map.136) | data formatting | bytes 4194304

commit v2 on v1

--- a/solution.py
+++ b/solution.py
@@ -49,6 +49,7 @@
     conv_out_ref,
     memory_out_ref,
     out_ref,
+    spilled_ref,
     tok,
     passages,
     in_weight,
@@ -63,7 +64,9 @@
     target,
     *rest,
 ):
-    owners, team, heads, capacity, rows, feat = sizes
+    owners, team, heads, capacity, direct, extra, rows, feat = sizes
+    rest_slots = capacity - direct
+    parts = 2 * heads
     chips = team // CORES
     own_rows = rows // team
     chunks = rows // SEQ_LEN
@@ -71,6 +74,9 @@
     table = [next(refs) for _ in range(2 * heads)]
     staged = [next(refs) for _ in range(2 * heads)]
     served = [next(refs) for _ in range(2 * heads)]
+    spill_out = [next(refs) for _ in range(2 * heads)] if extra else None
+    spill_in = [next(refs) for _ in range(2 * heads)] if extra else None
+    packed = [next(refs) for _ in range(2 * heads)] if extra else None
     branch = [next(refs) for _ in range(2 * heads)]
     moved = [next(refs) for _ in range(2 * heads)]
     (
@@ -97,14 +103,19 @@
         w_side_recv,
         w_pass_send,
         w_pass_recv,
+        spill_send,
+        spill_recv,
+        packed_send,
+        packed_recv,
     ) = refs
 
     st = lax.axis_index("st")
     me = lax.axis_index("tp")
     chip, core = me // CORES, me % CORES
     partner = chip * CORES + 1 - core
-    side = flip(st, 1)
-    half = st % 2
+    mine_piece = st % parts
+    half = st // 4
+    beside = 1 - half
 
     def up(k):
         return lax.rem(chip + k, chips) * CORES + core
@@ -133,7 +144,7 @@
             loads.append(
                 (
                     ref.at[h * HEAD_SIZE : (h + 1) * HEAD_SIZE, :],
-                    out_weight.at[b, h, aligned(me, HEAD_SIZE), :],
+                    out_weight.at[b * heads + h, aligned(me, HEAD_SIZE), :],
                 )
             )
     loads = [pltpu.make_async_copy(s, d, load_sem.at[i]) for i, (s, d) in enumerate(loads)]
@@ -161,10 +172,19 @@
     requests = [(j, b) for j in range(NPB) for b in range(names_ref.shape[1])]
     filled = jnp.zeros((owners, LANES), jnp.int32)
     asks = jnp.zeros((owners, LANES), jnp.int32)
+    over = jnp.zeros((owners, LANES), jnp.int32)
     for j, b in requests:
         hit = row == names_ref[j, b]
         asks = jnp.where(hit & (lane == filled), slots_ref[j, b], asks)
+        if extra:
+            late = jnp.where(hit & (filled >= direct) & (row // 4 != half), 1, 0)
+            entry = (row % 4) * (2 * rest_slots) + filled - direct
+            entry = jnp.sum(late * entry, axis=0, keepdims=True)
+            late = jnp.sum(late, axis=0, keepdims=True)
+            asks = jnp.where((late > 0) & (lane == capacity + over), entry, asks)
+            over = over + late
         filled = jnp.where(hit, filled + 1, filled)
+    asks = jnp.where(lane == LANES - 1, over, asks)
     for o in range(owners):
         asked[o, 0:1, :] = asks[o : o + 1, :]
 
@@ -238,21 +258,42 @@
         )
 
     def w_near(owner):
-        place = out_weight.at[:, :, aligned(owner, HEAD_SIZE), :]
+        place = out_weight.at[:, aligned(owner, HEAD_SIZE), :]
         return remote(place, place, w_near_send, w_near_recv, (st, partner))
 
+    def w_place(which, owner):
+        return out_weight.at[which, aligned(owner, HEAD_SIZE), :]
+
     def w_far(k, owner):
-        place = out_weight.at[half, :, aligned(owner, HEAD_SIZE), :]
+        place = w_place(mine_piece, owner)
         return remote(place, place, w_far_send.at[k - 1], w_far_recv.at[k - 1], (st, up(k)))
 
-    def w_side(k, owner, which):
-        place = out_weight.at[which, :, aligned(owner, HEAD_SIZE), :]
-        return remote(place, place, w_side_send.at[k - 1], w_side_recv.at[k - 1], (side, me))
-
-    def w_pass(j, k, owner, which):
-        place = out_weight.at[which, :, aligned(owner, HEAD_SIZE), :]
-        return remote(
-            place, place, w_pass_send.at[j, k - 1], w_pass_recv.at[j, k - 1], (st, partner)
+    def w_side(m, k, which):
+        place = w_place(which, down(k))
+        return remote(
+            place,
+            place,
+            w_side_send.at[m, k - 1],
+            w_side_recv.at[m, k - 1],
+            (flip(st, 1 if m == 3 else m), me),
+        )
+
+    def w_piece(m):
+        return lax.rem(flip(st, m), parts) if m else mine_piece
+
+    def w_sent(m):
+        return w_piece(2) if m == 3 else mine_piece
+
+    def w_turn():
+        for k in range(1, chips):
+            w_side(2, k, w_piece(2)).wait_recv()
+            w_side(3, k, w_sent(3)).start()
+            w_pass(2, k, down(k)).start()
+
+    def w_pass(m, k, owner):
+        place = w_place(w_piece(m), owner)
+        return remote(
+            place, place, w_pass_send.at[m, k - 1], w_pass_recv.at[m, k - 1], (st, partner)
         )
 
     for copy in loads[token_loads:]:
@@ -268,19 +309,95 @@
         near_copy(c, me).start()
 
     def serve(i, m, slot):
-        return remote(
-            staged[i].at[flip(st, m)],
-            served[i].at[aligned(slot, capacity)],
+        count = direct if m >= 4 else capacity
+        return remote(
+            staged[i].at[flip(st, m), 0:count],
+            served[i].at[pl.ds(slot * capacity, count)],
             serve_send.at[i, m],
             serve_recv.at[i, m],
             (flip(st, m), me),
         )
 
+    def beside_middle(j):
+        return j + 2 * beside + 4 * half
+
+    def spill(i, j):
+        return remote(
+            spill_out[i].at[j],
+            spill_in[i].at[pl.ds((st % 4) * 2 * rest_slots, 2 * rest_slots)],
+            spill_send.at[i, j],
+            spill_recv.at[i, st % 4],
+            (beside_middle(j), me),
+        )
+
+    def spill_arrival(i, source):
+        return remote(
+            spill_out[i].at[0],
+            spill_in[i].at[pl.ds(source * 2 * rest_slots, 2 * rest_slots)],
+            spill_send.at[i, 0],
+            spill_recv.at[i, source],
+            (source + 4 * half, me),
+        )
+
+    def far_reader(j, t):
+        return j + 2 * t + 4 * beside
+
+    def start_spill(i):
+        for j in range(2):
+            here = beside_middle(j) == st
+            for t in range(2):
+                for c in range(rest_slots):
+                    found = table[i][wanted[far_reader(j, t), 0, direct + c]]
+                    spill_out[i][j, t * rest_slots + c] = found
+
+            @pl.when(here)
+            def _():
+                for n in range(2 * rest_slots):
+                    spill_in[i][(st % 4) * 2 * rest_slots + n] = spill_out[i][j, n]
+
+            @pl.when(jnp.logical_not(here))
+            def _():
+                spill(i, j).start()
+
+    def packed_copy(i, t):
+        return remote(
+            packed[i].at[t],
+            served[i].at[pl.ds(owners * capacity, extra)],
+            packed_send.at[i, t],
+            packed_recv.at[i],
+            (far_reader(st % 2, t), me),
+        )
+
+    is_beside = (st // 2) % 2 == beside
+
+    def relay(i):
+        @pl.when(is_beside)
+        def _():
+            for source in range(4):
+
+                @pl.when(source != st % 4)
+                def _():
+                    spill_arrival(i, source).wait_recv()
+
+            for t in range(2):
+                for n in range(extra):
+                    entry = wanted[far_reader(st % 2, t), 0, capacity + n]
+                    packed[i][t, n] = spill_in[i][entry + t * rest_slots]
+            for t in range(2):
+                packed_copy(i, t).start()
+
+    def wait_served(i):
+        for m in range(1, owners):
+            serve(i, m, flip(st, m)).wait_recv()
+        if extra:
+            packed_copy(i, 0).wait_recv()
+
     def pass_weights():
         for k in range(1, chips):
             w_far(k, down(k)).wait_recv()
-            w_side(k, down(k), half).start()
-            w_pass(0, k, down(k), half).start()
+            for m in range(1, min(parts, 3)):
+                w_side(m, k, mine_piece).start()
+            w_pass(0, k, down(k)).start()
 
     project_half(1)
     for copy in loads[2:token_loads]:
@@ -296,12 +413,18 @@
             loads[2 * h + 1].wait()
             for i in range(pieces):
                 project(h, i)
+        if extra:
+            for i in (2 * h, 2 * h + 1):
+                start_spill(i)
+            if h == 1:
+                relay(0)
+                relay(1)
         if h == 1:
             pass_weights()
         for i in (2 * h, 2 * h + 1):
             for m in range(owners - 1, 0, -1):
                 reader = flip(st, m)
-                for c in range(capacity):
+                for c in range(direct if m >= 4 else capacity):
                     staged[i][reader, c] = table[i][wanted[reader, 0, c]]
                 if m < owners - 1:
                     serve(i, m + 1, st).start()
@@ -311,21 +434,34 @@
     if heads == 1:
         pass_weights()
 
+    late = jnp.int32(0)
     for f, (j, b) in enumerate(requests):
         name = names_ref[j, b]
-        place = name * capacity
+        place = jnp.int32(0)
         for i, a in requests[:f]:
             place = place + jnp.where(names_ref[i, a] == name, 1, 0)
-        target[b * NPB + j] = place
+        where = name * capacity + place
+        if extra:
+            is_late = jnp.logical_and(place >= direct, name // 4 != half)
+            where = jnp.where(is_late, owners * capacity + jnp.minimum(late, extra - 1), where)
+            late = late + jnp.where(is_late, 1, 0)
+        target[b * NPB + j] = where
+    most = late
+    for m in range(1, owners):
+        most = jnp.maximum(most, wanted[flip(st, m), 0, LANES - 1])
+    spilled_ref[0] = most
 
     for copy in loads[kv_loads:token_loads]:
         copy.wait()
 
+    turn = chunks - 2
     row_number = lax.broadcasted_iota(jnp.int32, (SEQ_LEN, 1), 0)
     taps = taps_ref[...].astype(jnp.float32)
 
     @pl.loop(0, chunks)
     def _(c):
+        if parts == 4:
+            pl.when(c == turn)(w_turn)
         for k in range(1, chips):
             far_copy(k, c, down(k)).wait_recv()
             pass_copy(k, c, down(k)).start()
@@ -348,6 +484,10 @@
         for h in range(heads):
             branch[h][here, :] = conv[:, h * HEAD_SIZE : (h + 1) * HEAD_SIZE]
 
+    if extra:
+        for i in range(2 if heads > 1 else 0, parts):
+            relay(i)
+
     others = [place(k) for k in range(1, chips) for place in (down, down_other)] + [partner]
 
     def row_send_copy(i, owner):
@@ -393,7 +533,7 @@
 
     blocks = own_rows // BLOCK
     tile = 512
-    tiles = out_weight.shape[3] // tile
+    tiles = out_weight.shape[2] // tile
 
     ones = jnp.ones((NPB * PLEN, HEAD_SIZE), jnp.bfloat16)
 
@@ -436,15 +576,13 @@
                     both[:, :HEAD_SIZE] / both[:, HEAD_SIZE:]
                 ).astype(jnp.bfloat16)
 
-        for m in range(1, owners):
-            serve(2 * h, m, flip(st, m)).wait_recv()
+        wait_served(2 * h)
 
         @pl.loop(0, team)
         def _(owner):
             owner_powers(owner)
 
-        for m in range(1, owners):
-            serve(2 * h + 1, m, flip(st, m)).wait_recv()
+        wait_served(2 * h + 1)
         for owner in others:
             owner_rows(owner)
             row_send_copy(heads + h, owner).start()
@@ -459,7 +597,7 @@
                 rows_of = aligned(lax.rem(chip + k, chips), CORES * HEAD_SIZE)
                 value = value + gates[:, 1:2] * jnp.dot(
                     moved[heads + h][:, rows_of],
-                    out_weight[1, h, rows_of, lanes],
+                    out_weight[heads + h, rows_of, lanes],
                     preferred_element_type=jnp.float32,
                 )
             if last:
@@ -474,10 +612,24 @@
             pl.loop(0, tiles)(add_tile)
 
     for k in range(1, chips):
-        w_side(k, down(k), 1 - half).wait_recv()
-        w_pass(1, k, down(k), 1 - half).start()
+        for m in range(1, parts):
+            if m != 2:
+                w_side(m, k, w_piece(m)).wait_recv()
+                w_pass(m, k, down(k)).start()
 
     def drain():
+        for i in range(parts if extra else 0):
+            for j in range(2):
+
+                @pl.when(beside_middle(j) != st)
+                def _():
+                    spill(i, j).wait_send()
+
+            @pl.when(is_beside)
+            def _():
+                for t in range(2):
+                    packed_copy(i, t).wait_send()
+
         for m in range(1, owners):
             ask(m, st).wait_send()
             for i in range(2 * heads):
@@ -492,9 +644,10 @@
 
         for k in range(1, chips):
             w_far(k, me).wait_send()
-            w_side(k, down(k), half).wait_send()
-            w_pass(0, k, down(k), half).wait_send()
-            w_pass(1, k, down(k), 1 - half).wait_send()
+            for m in range(parts):
+                if m:
+                    w_side(m, k, w_sent(m)).wait_send()
+                w_pass(m, k, down(k)).wait_send()
         w_near(me).wait_send()
 
     for h in range(heads):
@@ -502,8 +655,8 @@
         if h == 0:
             w_near(partner).wait_recv()
             for k in range(1, chips):
-                w_pass(0, k, down_other(k), half).wait_recv()
-                w_pass(1, k, down_other(k), 1 - half).wait_recv()
+                for m in range(parts):
+                    w_pass(m, k, down_other(k)).wait_recv()
             for i in range(heads):
                 wait_rows(i)
 
@@ -514,7 +667,7 @@
                 for i in range(heads):
                     value = value + jnp.dot(
                         moved[i][...],
-                        out_weight[0, i, :, lanes],
+                        out_weight[i, :, lanes],
                         preferred_element_type=jnp.float32,
                     )
                 total[:, lanes] = gates[:, 0:1] * value
@@ -535,7 +688,8 @@
             row_send_copy(i, owner).wait_send()
 
 
-def local(
+def fused(
+    spills,
     tokens,
     store,
     passage_holder_index,
@@ -564,6 +718,10 @@
 
     count = passage_holder_index.size
     capacity = max(2, 2 * count // owners)
+    direct, extra = capacity, 0
+    if spills:
+        direct = (5 * capacity + 7) // 8
+        extra = count * 3 // 16
     flat_rows = store.reshape(-1, store.shape[-1])
     held = store.shape[0]
     bf16, f32 = jnp.bfloat16, jnp.float32
@@ -573,7 +731,7 @@
         pltpu.VMEM(flat_rows.shape, bf16),
         pltpu.VMEM((4, team * feat, head_width), bf16),
         pltpu.VMEM((heads, team * feat, 2 * HEAD_SIZE), bf16),
-        pltpu.VMEM((2, heads, depth, width), bf16),
+        pltpu.VMEM((2 * heads, depth, width), bf16),
         pltpu.VMEM((own_rows, width), f32),
         pltpu.VMEM((rows, head_width), bf16),
         pltpu.VMEM((own_rows, 2), f32),
@@ -584,7 +742,12 @@
     ]
     scratch += [pltpu.VMEM((held, PLEN, HEAD_SIZE), bf16)] * (2 * heads)
     scratch += [pltpu.VMEM((owners, capacity, PLEN, HEAD_SIZE), bf16)] * (2 * heads)
-    scratch += [pltpu.VMEM((owners * capacity, PLEN, HEAD_SIZE), bf16)] * (2 * heads)
+    scratch += [pltpu.VMEM((owners * capacity + extra, PLEN, HEAD_SIZE), bf16)] * (2 * heads)
+    if spills:
+        rest_slots = capacity - direct
+        scratch += [pltpu.VMEM((2, 2 * rest_slots, PLEN, HEAD_SIZE), bf16)] * (2 * heads)
+        scratch += [pltpu.VMEM((8 * rest_slots, PLEN, HEAD_SIZE), bf16)] * (2 * heads)
+        scratch += [pltpu.VMEM((2, extra, PLEN, HEAD_SIZE), bf16)] * (2 * heads)
     scratch += [pltpu.VMEM((rows, HEAD_SIZE), bf16)] * (2 * heads)
     scratch += [pltpu.VMEM((own_rows, depth), bf16)] * (2 * heads)
     scratch += [
@@ -607,22 +770,29 @@
         dma,
         dma((chips - 1,)),
         dma((chips - 1,)),
-        dma((chips - 1,)),
-        dma((chips - 1,)),
-        dma((2, chips - 1)),
-        dma((2, chips - 1)),
+        dma((2 * heads, chips - 1)),
+        dma((2 * heads, chips - 1)),
+        dma((2 * heads, chips - 1)),
+        dma((2 * heads, chips - 1)),
+        dma((2 * heads, 2)),
+        dma((2 * heads, 4)),
+        dma((2 * heads, 2)),
+        dma((2 * heads,)),
     ]
     smem = pl.BlockSpec(memory_space=pltpu.SMEM)
     vmem = pl.BlockSpec(memory_space=pltpu.VMEM)
     hbm = pl.BlockSpec(memory_space=pltpu.HBM)
     return pl.pallas_call(
-        functools.partial(fused_kernel, (owners, team, heads, capacity, rows, feat)),
-        out_shape=pltpu.VMEM((own_rows, width), bf16),
+        functools.partial(fused_kernel, (owners, team, heads, capacity, direct, extra, rows, feat)),
+        out_shape=(
+            pltpu.VMEM((own_rows, width), bf16),
+            jax.ShapeDtypeStruct((1,), jnp.int32),
+        ),
         in_specs=[smem, smem] + [hbm] * 8 + [vmem, vmem] + [hbm] * 2,
-        out_specs=vmem,
+        out_specs=(vmem, smem),
         scratch_shapes=scratch,
         compiler_params=pltpu.CompilerParams(
-            collective_id=0, has_side_effects=True, vmem_limit_bytes=56 * 1024 * 1024
+            collective_id=int(spills), has_side_effects=True, vmem_limit_bytes=56 * 1024 * 1024
         ),
     )(
         passage_holder_index.T,
@@ -639,6 +809,16 @@
         route_gate_projection.T,
         conv_out,
         memory_out,
+    )
+
+
+def local(*args):
+    count, owners = args[2].size, lax.axis_size("st")
+    if owners != 8:
+        return fused(False, *args)[0]
+    result, most = fused(True, *args)
+    return lax.cond(
+        most[0] > count * 3 // 16, lambda: fused(False, *args)[0], lambda: result
     )
 
 

time: 112 us -> 105 us (0.938)
  the two profiles are of different devices: /device:TPU:0 before, /device:TPU:16 now
where the time goes in v2:
time: 105 us
  Pallas kernels  103 us (98%)
  local copies, waits for them, and re-layouts  1.35 us (1%)
    pallas_call x1, Pallas kernels, fused(): pl.pallas_call(functools.partial(fused_kernel, (owners, team, heads, capa...  103 us

profile of v2, /device:TPU:16, one launch (start us, length us, event | category | flops | bytes accessed | tf_op | source)
XLA Modules:
  0.0 105.1 jit_solution(11419843549820350213)
XLA Ops:
  0.0 0.0 copy-start
  0.0 0.0 copy-start.1
  0.0 0.0 copy-start.2
  0.0 0.0 copy-start.3
  0.0 0.0 copy-start.4
  0.0 0.0 copy-start.5
  0.0 0.0 copy-start.6
  0.0 0.0 copy-start.7
  0.1 102.8 %shard_map.138 = (bf16[512,2048]{1,0:T(8,128)(2,1)S(1)}, s32[1]{0:T(128)}) custom-call(s32[2,16]{1,0:T(2,128)} %bitcast.13, s32[2,16]{1,0:T(2,128)} %bitcast.15, bf16[2048,512]{1,0:T(8,128)(2,1)} %tokens_ref.1, bf16[2048,2048]{1,0:T(8,128)(2,1)} %bitcast.9, bf16[2048,256]{1,0:T(8,128)(2,1)} %key_ref.1, bf16[2048,256]{1,0:T(8,128)(2,1)} %value_ref.1, ...), custom_call_target="tpu_custom_call" | custom-call | tf_op jit(solution)/shard_map/pallas_call | solution.py:785
  103.5 0.0 copy-done
  103.5 0.0 copy-done.1
  103.6 0.0 copy-done.2
  103.6 0.0 copy-done.3
  103.6 0.0 copy-done.4
  103.6 0.0 copy-done.5
  103.6 0.0 copy-done.6
  103.6 0.0 copy-done.7
  103.6 0.2 conditional.1
  103.8 1.3 %copy.20 = bf16[512,2048]{1,0:T(8,128)(2,1)} copy(bf16[512,2048]{1,0:T(8,128)(2,1)S(1)} %get-tuple-element.56) | data formatting | bytes 4194304
Async XLA Ops:
  0.0 103.5 %copy-start = (bf16[2048,512]{1,0:T(8,128)(2,1)S(1)}, bf16[2048,512]{1,0:T(8,128)(2,1)}, u32[]{:S(2)}) copy-start(bf16[2048,512]{1,0:T(8,128)(2,1)} %tokens_ref.1) | copy-start | bytes 6291460
  0.0 103.5 %copy-start.1 = (bf16[2048,256]{1,0:T(8,128)(2,1)S(1)}, bf16[2048,256]{1,0:T(8,128)(2,1)}, u32[]{:S(2)}) copy-start(bf16[2048,256]{1,0:T(8,128)(2,1)} %key_ref.1) | copy-start | bytes 3145732
  0.0 103.6 %copy-start.2 = (bf16[2048,256]{1,0:T(8,128)(2,1)S(1)}, bf16[2048,256]{1,0:T(8,128)(2,1)}, u32[]{:S(2)}) copy-start(bf16[2048,256]{1,0:T(8,128)(2,1)} %value_ref.1) | copy-start | bytes 3145732
  0.0 103.6 %copy-start.3 = (bf16[2048,256]{1,0:T(8,128)(2,1)S(1)}, bf16[2048,256]{1,0:T(8,128)(2,1)}, u32[]{:S(2)}) copy-start(bf16[2048,256]{1,0:T(8,128)(2,1)} %query_ref.1) | copy-start | bytes 3145732
  0.0 103.6 %copy-start.4 = (bf16[2048,2]{0,1:T(2,128)(2,1)S(1)}, bf16[2048,2]{0,1:T(2,128)(2,1)}, u32[]{:S(2)}) copy-start(bf16[2048,2]{0,1:T(2,128)(2,1)} %param.27) | copy-start | bytes 24580
  0.0 103.6 %copy-start.5 = (bf16[3,256]{1,0:T(4,128)(2,1)S(1)}, bf16[3,256]{1,0:T(4,128)(2,1)}, u32[]{:S(2)}) copy-start(bf16[3,256]{1,0:T(4,128)(2,1)} %taps_ref.1) | copy-start | bytes 4612
  0.0 103.6 %copy-start.6 = (s32[16,2]{0,1:T(2,128)S(1)}, s32[16,2]{0,1:T(2,128)}, u32[]{:S(2)}) copy-start(s32[16,2]{0,1:T(2,128)} %param.18) | copy-start | bytes 388
  0.0 103.6 %copy-start.7 = (s32[16,2]{0,1:T(2,128)S(1)}, s32[16,2]{0,1:T(2,128)}, u32[]{:S(2)}) copy-start(s32[16,2]{0,1:T(2,128)} %param.19) | copy-start | bytes 388

commit v3 on v2

--- a/solution.py
+++ b/solution.py
@@ -786,13 +786,13 @@
         functools.partial(fused_kernel, (owners, team, heads, capacity, direct, extra, rows, feat)),
         out_shape=(
             pltpu.VMEM((own_rows, width), bf16),
-            jax.ShapeDtypeStruct((1,), jnp.int32),
+            pltpu.SMEM((1,), jnp.int32),
         ),
         in_specs=[smem, smem] + [hbm] * 8 + [vmem, vmem] + [hbm] * 2,
         out_specs=(vmem, smem),
         scratch_shapes=scratch,
         compiler_params=pltpu.CompilerParams(
-            collective_id=int(spills), has_side_effects=True, vmem_limit_bytes=56 * 1024 * 1024
+            collective_id=int(spills), has_side_effects=True, vmem_limit_bytes=61 * 1024 * 1024
         ),
     )(
         passage_holder_index.T,

time: 105 us -> 103 us (0.981)
  the two profiles are of different devices: /device:TPU:16 before, /device:TPU:0 now
where the time goes in v3:
time: 103 us; the launch traced here: 102 us
  Pallas kernels  100 us (97%)
  local copies, waits for them, and re-layouts  1.34 us (1%)
    pallas_call x1, Pallas kernels, fused(): pl.pallas_call(functools.partial(fused_kernel, (owners, team, heads, capa...  100 us

profile of v3, /device:TPU:0, one launch (start us, length us, event | category | flops | bytes accessed | tf_op | source)
XLA Modules:
  0.0 101.8 jit_solution(12911721854825519921)
XLA Ops:
  0.0 0.0 copy-start
  0.0 0.0 copy-start.1
  0.0 0.0 copy-start.2
  0.0 0.0 copy-start.3
  0.0 100.2 %shard_map.138 = (bf16[512,2048]{1,0:T(8,128)(2,1)S(1)}, s32[1]{0:T(128)S(4)}) custom-call(s32[2,16]{1,0:T(2,128)} %bitcast.13, s32[2,16]{1,0:T(2,128)} %bitcast.15, bf16[2048,512]{1,0:T(8,128)(2,1)} %tokens_ref.1, bf16[2048,2048]{1,0:T(8,128)(2,1)} %bitcast.9, bf16[2048,256]{1,0:T(8,128)(2,1)} %key_ref.1, bf16[2048,256]{1,0:T(8,128)(2,1)} %value_ref.1, ...), custom_call_target="tpu_custom_call" | custom-call | tf_op jit(solution)/shard_map/pallas_call | solution.py:785
  100.2 0.0 copy-done
  100.2 0.0 copy-done.1
  100.3 0.0 copy-done.2
  100.3 0.0 copy-done.3
  100.3 0.2 conditional.1
  100.5 1.3 %copy.20 = bf16[512,2048]{1,0:T(8,128)(2,1)} copy(bf16[512,2048]{1,0:T(8,128)(2,1)S(1)} %get-tuple-element.56) | data formatting | bytes 4194304
Async XLA Ops:
  0.0 100.2 %copy-start = (bf16[2048,2]{0,1:T(2,128)(2,1)S(1)}, bf16[2048,2]{0,1:T(2,128)(2,1)}, u32[]{:S(2)}) copy-start(bf16[2048,2]{0,1:T(2,128)(2,1)} %param.27) | copy-start | bytes 24580
  0.0 100.2 %copy-start.1 = (bf16[3,256]{1,0:T(4,128)(2,1)S(1)}, bf16[3,256]{1,0:T(4,128)(2,1)}, u32[]{:S(2)}) copy-start(bf16[3,256]{1,0:T(4,128)(2,1)} %taps_ref.1) | copy-start | bytes 4612
  0.0 100.3 %copy-start.2 = (s32[16,2]{0,1:T(2,128)S(1)}, s32[16,2]{0,1:T(2,128)}, u32[]{:S(2)}) copy-start(s32[16,2]{0,1:T(2,128)} %param.18) | copy-start | bytes 388
  0.0 100.3 %copy-start.3 = (s32[16,2]{0,1:T(2,128)S(1)}, s32[16,2]{0,1:T(2,128)}, u32[]{:S(2)}) copy-start(s32[16,2]{0,1:T(2,128)} %param.19) | copy-start | bytes 388
